TPU v7x, 512 devices: a whole 4x4x16 slice. The times are simulated.
512 devices in a mesh: ep: 16 (over y, x), tp: 32 (over z, core).
Axes of the slice: x: 4, y: 4, z: 16, core: 2. Of those that a mesh axis runs over, the one named last changes fastest.
Arguments:
- tokens: bfloat16 [8192, 4096], P('tp', 'ep'), may hold values from -20 to 20
- norm_gain: bfloat16 [4096], P('ep'), may hold values from 0.099609375 to 1.8984375
- expert_ids: int32 [8192, 2], P('tp'), may hold values from 0 to 31, all different within a row; in each aligned block of 256 rows (0 to 255, 256 to 511, ...) at most 32 rows name the same one
- combine_weight: float32 [8192, 2], P('tp'), may hold values from 0.05 to 1
- w_gate: bfloat16 [32, 2048, 4096], P('tp', 'ep'), may hold values from -0.09375 to 0.09375
- w_up: bfloat16 [32, 2048, 4096], P('tp', 'ep'), may hold values from -0.09375 to 0.09375
- w_down: bfloat16 [32, 2048, 4096], P('tp', None, 'ep'), may hold values from -2 to 2
- out_gain: bfloat16 [4096], P('ep'), may hold values from 0.099609375 to 1.8984375
Outputs:
- mixed: bfloat16 [8192, 4096], P('tp', 'ep')
Inputs may be any that keep to these rules, and one draw needn't show every extreme that they name: `expert_ids`: each row names 2 different experts; among the rows of one index of tp no expert is named by more than 32 rows, a bound that some block reaches.
All inputs are finite; a program needn't handle non-finite values.
Results may differ from a plain program's by a relative error of at most 0.007.
Values may be sent and summed in bfloat16 or wider, within the bound.
No kernel may reach another device: no remote copies, remote signals or barrier semaphores. Data moves between devices by JAX's collectives and lax.ppermute only.
A program may use at most 64 MiB of HBM per device.

v0:
```python
import jax
import jax.numpy as jnp
from jax import lax
from jax.sharding import Mesh
from jax.sharding import PartitionSpec as P

TP = ("tp_0", "tp_1")
epsilon = 1e-06


def sent_to_all(value, axis):
    copies = jnp.broadcast_to(value, (lax.axis_size(axis), *value.shape))
    return lax.all_to_all(copies, axis, split_axis=0, concat_axis=0, tiled=True)


def over_copies(value, axis):
    everything = sent_to_all(value, axis)
    return jnp.sum(everything, axis=0)


def cut_along(value, dim, peers):
    before, after = (value.shape[:dim], value.shape[dim + 1 :])
    return jnp.moveaxis(value.reshape(*before, peers, -1, *after), dim, 0)


def in_order(parts, dim):
    parts = jnp.moveaxis(parts, 0, dim)
    lengths = parts.shape
    return parts.reshape(*lengths[:dim], lengths[dim] * lengths[dim + 1], *lengths[dim + 2 :])


def turned_blocks(parts, axes, turns):
    lengths = [lax.axis_size(a) for a in axes]
    parts = parts.reshape(*lengths, *parts.shape[1:])
    for k in turns:
        parts = lax.all_to_all(parts, axes[k], split_axis=k, concat_axis=k, tiled=True)
    return parts.reshape(-1, *parts.shape[len(axes) :])


def core_and_chips(value, groups, turns, split_dim, concat_dim):
    peers = lax.axis_size(groups[0]) * lax.axis_size(groups[1])
    parts = cut_along(value, split_dim, peers)
    return in_order(turned_blocks(parts, groups, turns), concat_dim)


def body(tokens, norm_gain, expert_ids, combine_weight, w_gate, w_up, w_down, out_gain):
    tok_rows, width_local = tokens.shape
    n_split = lax.axis_size("ep")
    n_route = lax.axis_size(TP)
    width = width_local * n_split
    local_experts = w_gate.shape[0]
    total_experts = local_experts * n_route
    top = expert_ids.shape[1]
    capacity = 2 * top * tok_rows // total_experts
    flat_ids = expert_ids.reshape(-1)
    onehot = (flat_ids[:, None] == jnp.arange(total_experts, dtype=jnp.int32)[None, :]).astype(
        jnp.int32
    )
    ranks = jnp.sum((jnp.cumsum(onehot, axis=0) - 1) * onehot, axis=1)
    target = flat_ids * capacity + ranks
    source_rows = jnp.arange(tok_rows * top, dtype=jnp.int32) // top
    xf = tokens.astype(jnp.float32)
    squares = over_copies(jnp.sum(xf * xf, axis=1), "ep")
    normed = (
        xf * lax.rsqrt(squares / width + epsilon)[:, None] * norm_gain.astype(jnp.float32)[None, :]
    ).astype(jnp.bfloat16)
    buffer = (
        jnp.zeros((total_experts * capacity, width_local), jnp.bfloat16)
        .at[target]
        .set(normed[source_rows])
    )
    arrived = lax.all_to_all(buffer, TP, split_axis=0, concat_axis=0, tiled=True)
    arrived = arrived.reshape(n_route, local_experts, capacity, width_local)
    piece = lax.all_gather(arrived, "ep", axis=3, tiled=True)
    gate_sum = jnp.einsum("sect,eft->secf", piece, w_gate, preferred_element_type=jnp.float32)
    up_sum = jnp.einsum("sect,eft->secf", piece, w_up, preferred_element_type=jnp.float32)
    hidden = (jax.nn.silu(gate_sum) * up_sum).astype(jnp.bfloat16)
    result = jnp.einsum(
        "secf,efd->secd",
        lax.all_gather(hidden, "ep", axis=3, tiled=True),
        w_down,
        preferred_element_type=jnp.float32,
    )
    expert_out = result.astype(jnp.bfloat16).reshape(
        n_route * local_experts * capacity, width_local
    )
    returned = core_and_chips(expert_out, ("tp_0", "tp_1"), (1, 0), 0, 0)
    picked = returned[target].astype(jnp.float32).reshape(tok_rows, top, width_local)
    moe = jnp.sum(picked * combine_weight[:, :, None], axis=1)
    squares_out = over_copies(jnp.sum(moe * moe, axis=1), "ep")
    mixed = (
        moe
        * lax.rsqrt(squares_out / width + epsilon)[:, None]
        * out_gain.astype(jnp.float32)[None, :]
    )
    return mixed.astype(jnp.bfloat16)


def solution(mesh):
    finer = Mesh(mesh.devices.reshape(mesh.shape["ep"], 16, 2), ("ep", "tp_0", "tp_1"))
    return jax.shard_map(
        body,
        mesh=finer,
        in_specs=(
            P(TP, "ep"),
            P("ep"),
            P(TP, None),
            P(TP, None),
            P(TP, "ep", None),
            P(TP, "ep", None),
            P(TP, None, "ep"),
            P("ep"),
        ),
        out_specs=P(TP, "ep"),
        check_vma=False,
    )
```

profile of v0, /device:TPU:32, one launch (start us, length us, event | category | flops | bytes accessed | tf_op | source)
XLA Modules:
  0.0 313.2 jit_solution(1302803057971697116)
XLA Ops:
  6.5 0.0 copy-start
  6.5 1.1 fusion.10
  7.6 0.6 broadcast_in_dim.7
  8.3 7.0 %all-to-all-start = ((f32[16,1,256]{2,1,0:T(1,128)}), f32[16,1,256]{2,1,0:T(1,128)S(1)}, u32[]{:S(2)}, u32[]{:S(2)}) async-start(f32[16,1,256]{2,1,0:T(1,128)} %broadcast_in_dim.7), calls=%async_computation | async-start | bytes 32768 | tf_op jit(solution)/shard_map/all_to_all | solution.py:13
  15.3 0.0 all-gather.6.cloned.1.call-start
  15.4 0.8 copy.37
  16.2 0.1 eq.29
  16.3 0.1 eq.25
  16.5 0.7 broadcast_multiply_fusion
  17.2 1.2 reduce-window.6
  18.3 0.2 slice_reduce_fusion
  18.6 0.1 copy.36
  18.8 0.1 mul.74
  18.9 0.1 fusion.17
  19.0 0.7 convert_element_type.44
  19.7 3.2 %all-to-all-done = f32[16,1,256]{2,1,0:T(1,128)S(1)} async-done(((f32[16,1,256]{2,1,0:T(1,128)}), f32[16,1,256]{2,1,0:T(1,128)S(1)}, u32[]{:S(2)}, u32[]{:S(2)}) %all-to-all-start) | async-done | bytes 16416 | tf_op jit(solution)/shard_map/all_to_all | solution.py:13
  22.9 1.0 fusion.12
  24.0 3.9 %scatter_custom_fusion = bf16[1024,256]{1,0:T(8,128)(2,1)S(1)} fusion(s32[512]{0:T(512)S(1)} %bitcast.65, bf16[256,256]{1,0:T(8,128)(2,1)S(1)} %fusion.12, s32[1024]{0:T(1024)S(1)} %pad_clamp_fusion.1, bf16[]{:T(256)} %constant.32.clone.1), kind=kCustom, calls=%fused_computation.19 | custom fusion | bytes 524290 | tf_op jit(solution)/shard_map/scatter | solution.py:70
  27.9 47.4 %all_to_all.31 = bf16[32,32,256]{2,1,0:T(8,128)(2,1)} all-to-all(bf16[32,32,256]{2,1,0:T(8,128)(2,1)S(1)} %bitcast.63), channel_id=1, replica_groups=mesh['ep'=16,'tp_0'=16,'tp_1'=2] {'tp_0','tp_1'}, dimensions={0} | all-to-all | bytes 1048576 | tf_op jit(solution)/shard_map/all_to_all | solution.py:72
  75.3 0.0 copy-start.3
  75.3 0.0 all-gather.6.cloned.1.call-update
  75.4 0.0 all-gather.4.cloned.1.call-start
  75.4 82.4 %all-gather.6.cloned.1.call-done = bf16[32,32,4096]{2,1,0:T(8,128)(2,1)} async-done(((bf16[32,32,256]{2,1,0:T(8,128)(2,1)}), bf16[32,32,4096]{2,1,0:T(8,128)(2,1)}) %all-gather.6.cloned.1.call-update) | async-done | bytes 8388624 | tf_op jit(solution)/shard_map/all_gather | solution.py:74
  157.9 0.0 copy-start.2
  157.9 6.1 %convolution_bitcast_fusion.1 = f32[32,1,32,128]{3,2,0,1:T(8,128)S(1)} fusion(bf16[32,32,4096]{2,1,0:T(8,128)(2,1)} %all-gather.6.cloned.1.call-done, bf16[1,128,4096]{2,1,0:T(8,128)(2,1)} %param.12), kind=kOutput, calls=%fused_computation.8 | convolution fusion | flops 1073741824 | bytes 9961472 | tf_op jit(solution)/shard_map/sect,eft->secf/dot_general | solution.py:75
  164.0 0.0 copy-done.3
  164.0 0.0 copy-done.2
  164.0 3.0 fusion.6
  167.0 0.0 copy-start.1
  167.0 0.0 copy-start.4
  167.0 0.0 all-gather.4.cloned.1.call-update
  167.0 71.7 %all-gather.4.cloned.1.call-done = bf16[32,1,32,2048]{3,2,0,1:T(8,128)(2,1)} async-done(((bf16[32,1,32,128]{3,2,0,1:T(8,128)(2,1)}), bf16[32,1,32,2048]{3,2,0,1:T(8,128)(2,1)}) %all-gather.4.cloned.1.call-update) | async-done | bytes 4194320 | tf_op jit(solution)/shard_map/all_gather | solution.py:80
  238.8 0.0 copy-done
  238.8 3.4 %fusion.2 = bf16[32,32,256]{2,1,0:T(8,128)(2,1)S(1)} fusion(bf16[32,1,32,2048]{3,2,0,1:T(8,128)(2,1)} %all-gather.4.cloned.1.call-done, bf16[1,2048,256]{2,1,0:T(8,128)(2,1)S(1)} %copy-done), kind=kOutput, calls=%fused_computation.5 | convolution fusion | flops 1074003968 | bytes 5767168 | tf_op jit(solution)/shard_map/secf,efd->secd/dot_general | solution.py:78
  242.3 4.2 %all_to_all.32 = bf16[16,2,32,256]{3,2,0,1:T(8,128)(2,1)S(1)} all-to-all(bf16[16,2,32,256]{3,2,0,1:T(8,128)(2,1)S(1)} %copy.41), channel_id=1, replica_groups=mesh['ep'=16,'tp_0'=16,'tp_1'=2] {'tp_1'}, dimensions={1} | all-to-all | bytes 1048576 | tf_op jit(solution)/shard_map/all_to_all | solution.py:36
  246.4 0.8 copy.42
  247.3 12.7 %all-to-all-start.3 = ((bf16[16,2,32,256]{3,2,1,0:T(8,128)(2,1)}), bf16[16,2,32,256]{3,2,1,0:T(8,128)(2,1)S(1)}, u32[]{:S(2)}, u32[]{:S(2)}) async-start(bf16[16,2,32,256]{3,2,1,0:T(8,128)(2,1)} %copy.42), calls=%async_computation.3 | async-start | bytes 1048576 | tf_op jit(solution)/shard_map/all_to_all | solution.py:36
  259.9 0.0 copy-done.1
  259.9 0.1 copy.43
  260.1 29.2 %all-to-all-done.3 = bf16[16,2,32,256]{3,2,1,0:T(8,128)(2,1)S(1)} async-done(((bf16[16,2,32,256]{3,2,1,0:T(8,128)(2,1)}), bf16[16,2,32,256]{3,2,1,0:T(8,128)(2,1)S(1)}, u32[]{:S(2)}, u32[]{:S(2)}) %all-to-all-start.3) | async-done | bytes 524320 | tf_op jit(solution)/shard_map/all_to_all | solution.py:36
  289.3 1.9 gather_fusion
  291.3 0.3 reshape.149
  291.5 0.7 multiply_reduce_fusion
  292.2 0.1 multiply_reduce_fusion.1
  292.4 0.6 broadcast_in_dim.8
  293.0 4.9 %all-to-all-start.4 = ((f32[16,1,256]{2,1,0:T(1,128)}), f32[16,1,256]{2,1,0:T(1,128)S(1)}, u32[]{:S(2)}, u32[]{:S(2)}) async-start(f32[16,1,256]{2,1,0:T(1,128)} %broadcast_in_dim.8), calls=%async_computation.4 | async-start | bytes 32768 | tf_op jit(solution)/shard_map/all_to_all | solution.py:13
  297.9 0.0 copy-done.4
  297.9 7.6 %all-to-all-done.4 = f32[16,1,256]{2,1,0:T(1,128)S(1)} async-done(((f32[16,1,256]{2,1,0:T(1,128)}), f32[16,1,256]{2,1,0:T(1,128)S(1)}, u32[]{:S(2)}, u32[]{:S(2)}) %all-to-all-start.4) | async-done | bytes 16416 | tf_op jit(solution)/shard_map/all_to_all | solution.py:13
  305.6 0.8 multiply_convert_fusion
  (13 shorter events, 0.2 us)
Async XLA Ops:
  6.5 232.2 %copy-start = (bf16[1,2048,256]{2,1,0:T(8,128)(2,1)S(1)}, bf16[1,2048,256]{2,1,0:T(8,128)(2,1)}, u32[]{:S(2)}) copy-start(bf16[1,2048,256]{2,1,0:T(8,128)(2,1)} %param.14) | copy-start | bytes 3145732
  8.3 14.6 %all-to-all-start = ((f32[16,1,256]{2,1,0:T(1,128)}), f32[16,1,256]{2,1,0:T(1,128)S(1)}, u32[]{:S(2)}, u32[]{:S(2)}) async-start(f32[16,1,256]{2,1,0:T(1,128)} %broadcast_in_dim.7), calls=%async_computation | async-start | bytes 32768 | tf_op jit(solution)/shard_map/all_to_all | solution.py:13
  15.3 142.5 %all-gather.6.cloned.1.call-start = ((), (), s32[]{:S(2)}) async-start(), calls=%async_computation.6 | async-start | bytes 8912896 | tf_op jit(solution)/shard_map/all_gather | solution.py:74
  75.3 88.6 %copy-start.3 = (bf16[1,128,4096]{2,1,0:T(8,128)(2,1)S(1)}, bf16[1,128,4096]{2,1,0:T(8,128)(2,1)}, u32[]{:S(2)}) copy-start(bf16[1,128,4096]{2,1,0:T(8,128)(2,1)} %param.13) | copy-start | bytes 3145732
  75.4 163.4 %all-gather.4.cloned.1.call-start = ((), (), s32[]{:S(2)}) async-start(), calls=%async_computation.5 | async-start | bytes 4456448 | tf_op jit(solution)/shard_map/all_gather | solution.py:80
  157.9 6.1 %copy-start.2 = (bf16[32,32,4096]{2,1,0:T(8,128)(2,1)S(1)}, bf16[32,32,4096]{2,1,0:T(8,128)(2,1)}, u32[]{:S(2)}) copy-start(bf16[32,32,4096]{2,1,0:T(8,128)(2,1)} %all-gather.6.cloned.1.call-done) | copy-start | bytes 25165828
  167.0 92.9 %copy-start.1 = (f32[256,2]{0,1:T(2,128)S(1)}, f32[256,2]{0,1:T(2,128)}, u32[]{:S(2)}) copy-start(f32[256,2]{0,1:T(2,128)} %param.11) | copy-start | bytes 6148
  167.0 130.9 %copy-start.4 = (bf16[256]{0:T(256)(128)(2,1)S(1)}, bf16[256]{0:T(256)(128)(2,1)}, u32[]{:S(2)}) copy-start(bf16[256]{0:T(256)(128)(2,1)} %param.15) | copy-start | bytes 1540
  247.3 42.1 %all-to-all-start.3 = ((bf16[16,2,32,256]{3,2,1,0:T(8,128)(2,1)}), bf16[16,2,32,256]{3,2,1,0:T(8,128)(2,1)S(1)}, u32[]{:S(2)}, u32[]{:S(2)}) async-start(bf16[16,2,32,256]{3,2,1,0:T(8,128)(2,1)} %copy.42), calls=%async_computation.3 | async-start | bytes 1048576 | tf_op jit(solution)/shard_map/all_to_all | solution.py:36
  293.0 12.5 %all-to-all-start.4 = ((f32[16,1,256]{2,1,0:T(1,128)}), f32[16,1,256]{2,1,0:T(1,128)S(1)}, u32[]{:S(2)}, u32[]{:S(2)}) async-start(f32[16,1,256]{2,1,0:T(1,128)} %broadcast_in_dim.8), calls=%async_computation.4 | async-start | bytes 32768 | tf_op jit(solution)/shard_map/all_to_all | solution.py:13
Sparse Core Ops, SparseCore 0:
  75.5 82.3 all-gather.5
  167.2 71.5 all-gather.3
where the time goes:
time: 314 us; the launch traced here: 313 us
  waiting for transfers between devices  194 us (62%)
  blocking collectives  51.6 us (16%)
  starting transfers between devices  24.7 us (8%)
  between operations  13.6 us (4%)
  matrix products  12.6 us (4%)
  local copies, waits for them, and re-layouts  9.98 us (3%)
  other arithmetic  6.47 us (2%)
    all_gather x1, waiting for transfers between devices, body(): piece = lax.all_gather(arrived, 'ep', axis=3, tiled=True)  82.4 us
    all_gather x1, waiting for transfers between devices, body(): lax.all_gather(hidden, 'ep', axis=3, tiled=True)  71.7 us
    all_to_all x1, blocking collectives, body(): lax.all_to_all(buffer, TP, split_axis=0, concat_axis=0, tiled=True)  47.4 us
    all_to_all x1, waiting for transfers between devices, turned_blocks(): lax.all_to_all(parts, axes[k], split_axis=k, concat_axis=k, tiled=True)  29.2 us
    all_to_all x1, starting transfers between devices, turned_blocks(): lax.all_to_all(parts, axes[k], split_axis=k, concat_axis=k, tiled=True)  12.7 us
    all_to_all x2, starting transfers between devices, sent_to_all(): return lax.all_to_all(copies, axis, split_axis=0, concat_axis=0, tiled=True)  12 us
    all_to_all x2, waiting for transfers between devices, sent_to_all(): return lax.all_to_all(copies, axis, split_axis=0, concat_axis=0, tiled=True)  10.8 us
  transfers between devices with their start and end apart: 5, of which 5 were waited for; matrix products, arithmetic and copies ran while one was open for 1% of the time, Pallas kernels for 0%

commit v1 on v0

--- a/solution.py
+++ b/solution.py
@@ -71,7 +71,9 @@
     )
     arrived = lax.all_to_all(buffer, TP, split_axis=0, concat_axis=0, tiled=True)
     arrived = arrived.reshape(n_route, local_experts, capacity, width_local)
-    piece = lax.all_gather(arrived, "ep", axis=3, tiled=True)
+    piece = jnp.concatenate(
+        lax.all_to_all(jnp.stack([arrived] * lax.axis_size("ep")), "ep", 0, 0), axis=3
+    )
     gate_sum = jnp.einsum("sect,eft->secf", piece, w_gate, preferred_element_type=jnp.float32)
     up_sum = jnp.einsum("sect,eft->secf", piece, w_up, preferred_element_type=jnp.float32)
     hidden = (jax.nn.silu(gate_sum) * up_sum).astype(jnp.bfloat16)

time: 314 us -> 353 us (1.12)
  blocking collectives: 51.6 us -> 151 us
  waiting for transfers between devices: 194 us -> 104 us
  local copies, waits for them, and re-layouts: 9.98 us -> 39.9 us
    all_to_all x0 -> x1, blocking collectives: none -> 99.6 us  [body(): lax.all_to_all(jnp.stack([arrived] * lax.axis_size('ep')), 'ep', 0, 0)]
    all_gather x1 -> x0, waiting for transfers between devices: 82.4 us -> none  [body(): piece = lax.all_gather(arrived, 'ep', axis=3, tiled=True)]
    reshape x0 -> x1, local copies, waits for them, and re-layouts: none -> 15.1 us  [body(): jnp.concatenate(lax.all_to_all(jnp.stack([arrived] * lax.axis_size('ep'))...]
    another operation x1 -> x3, local copies, waits for them, and re-layouts: 0.01 us -> 14.6 us
    all_gather x1, waiting for transfers between devices: 71.7 us -> 63.9 us  [body(): lax.all_gather(hidden, 'ep', axis=3, tiled=True)]
  transfers between devices with their start and end apart: 5 -> 4, of which waited for: 5 -> 4; matrix products, arithmetic and copies ran while one was open for 1% -> 1% of each run, Pallas kernels for 0% -> 0%
where the time goes in v1:
time: 353 us; the launch traced here: 352 us
  blocking collectives  151 us (43%)
  waiting for transfers between devices  104 us (29%)
  local copies, waits for them, and re-layouts  39.9 us (11%)
  starting transfers between devices  24.7 us (7%)
  between operations  13.6 us (4%)
  matrix products  12.3 us (3%)
  other arithmetic  6.47 us (2%)
    all_to_all x1, blocking collectives, body(): lax.all_to_all(jnp.stack([arrived] * lax.axis_size('ep')), 'ep', 0, 0)  99.6 us
    all_gather x1, waiting for transfers between devices, body(): lax.all_gather(hidden, 'ep', axis=3, tiled=True)  63.9 us
    all_to_all x1, blocking collectives, body(): lax.all_to_all(buffer, TP, split_axis=0, concat_axis=0, tiled=True)  47.3 us
    all_to_all x1, waiting for transfers between devices, turned_blocks(): lax.all_to_all(parts, axes[k], split_axis=k, concat_axis=k, tiled=True)  29.2 us
    reshape x1, local copies, waits for them, and re-layouts, body(): jnp.concatenate(lax.all_to_all(jnp.stack([arrived] * lax.axis_size('ep'))...  15.1 us
    another operation x2, local copies, waits for them, and re-layouts  13.6 us
    all_to_all x1, starting transfers between devices, turned_blocks(): lax.all_to_all(parts, axes[k], split_axis=k, concat_axis=k, tiled=True)  12.7 us
    all_to_all x2, starting transfers between devices, sent_to_all(): return lax.all_to_all(copies, axis, split_axis=0, concat_axis=0, tiled=True)  12 us
  transfers between devices with their start and end apart: 4, of which 4 were waited for; matrix products, arithmetic and copies ran while one was open for 1% of the time, Pallas kernels for 0%

profile of v1, /device:TPU:32, one launch (start us, length us, event | category | flops | bytes accessed | tf_op | source)
XLA Modules:
  0.0 351.9 jit_solution(9600843970639325818)
XLA Ops:
  6.5 0.0 copy-start
  6.5 1.1 fusion.10
  7.6 0.6 broadcast_in_dim.7
  8.3 7.0 %all-to-all-start = ((f32[16,1,256]{2,1,0:T(1,128)}), f32[16,1,256]{2,1,0:T(1,128)S(1)}, u32[]{:S(2)}, u32[]{:S(2)}) async-start(f32[16,1,256]{2,1,0:T(1,128)} %broadcast_in_dim.7), calls=%async_computation | async-start | bytes 32768 | tf_op jit(solution)/shard_map/all_to_all | solution.py:13
  15.3 0.0 all-gather.2.cloned.1.call-start
  15.4 0.8 copy.40
  16.2 0.1 eq.29
  16.3 0.1 eq.25
  16.5 0.7 broadcast_multiply_fusion
  17.2 1.2 reduce-window.6
  18.3 0.2 slice_reduce_fusion
  18.6 0.1 copy.39
  18.8 0.1 mul.74
  18.9 0.1 fusion.17
  19.0 0.7 convert_element_type.44
  19.7 3.2 all-to-all-done
  22.9 1.0 fusion.12
  24.0 3.9 %scatter_custom_fusion = bf16[1024,256]{1,0:T(8,128)(2,1)S(1)} fusion(s32[512]{0:T(512)S(1)} %bitcast.71, bf16[256,256]{1,0:T(8,128)(2,1)S(1)} %fusion.12, s32[1024]{0:T(1024)S(1)} %pad_clamp_fusion.1, bf16[]{:T(256)} %constant.32.clone.1), kind=kCustom, calls=%fused_computation.19 | custom fusion | bytes 524290 | tf_op jit(solution)/shard_map/scatter | solution.py:70
  27.9 47.3 %all_to_all.36 = bf16[32,32,256]{2,1,0:T(8,128)(2,1)S(1)} all-to-all(bf16[32,32,256]{2,1,0:T(8,128)(2,1)S(1)} %bitcast.69), channel_id=1, replica_groups=mesh['ep'=16,'tp_0'=16,'tp_1'=2] {'tp_0','tp_1'}, dimensions={0} | all-to-all | bytes 1048576 | tf_op jit(solution)/shard_map/all_to_all | solution.py:72
  75.2 1.1 stack.3
  76.3 99.6 %all_to_all.37 = bf16[16,32,1,32,256]{4,3,1,2,0:T(8,128)(2,1)} all-to-all(bf16[16,32,1,32,256]{4,3,1,2,0:T(8,128)(2,1)S(1)} %stack.3), channel_id=1, replica_groups=mesh['ep'=16,'tp_0'=16,'tp_1'=2] {'ep'}, dimensions={0} | all-to-all | bytes 16777216 | tf_op jit(solution)/shard_map/all_to_all | solution.py:75
  175.9 15.1 %copy.44 = bf16[32,1,32,16,256]{4,3,2,0,1:T(8,128)(2,1)} copy(bf16[32,1,32,16,256]{4,2,0,1,3:T(8,128)(2,1)} %bitcast.67) | data formatting | bytes 16777216 | tf_op jit(solution)/shard_map/reshape | solution.py:74
  191.0 0.0 copy-start.3
  191.0 13.6 %reshape.149 = bf16[32,32,4096]{2,1,0:T(8,128)(2,1)} reshape(bf16[32,1,32,16,256]{4,3,2,0,1:T(8,128)(2,1)} %copy.44) | data formatting | bytes 16777216 | tf_op jit(solution)/shard_map/reshape.9
  204.6 0.0 copy-done.3
  204.6 0.0 copy-start.1
  204.6 0.0 copy-start.4
  204.6 5.9 %convolution_bitcast_fusion.1 = f32[32,1,32,128]{3,2,0,1:T(8,128)S(1)} fusion(bf16[32,32,4096]{2,1,0:T(8,128)(2,1)} %reshape.149, bf16[1,128,4096]{2,1,0:T(8,128)(2,1)S(1)} %copy-done.3), kind=kOutput, calls=%fused_computation.8 | convolution fusion | flops 1073741824 | bytes 9961472 | tf_op jit(solution)/shard_map/sect,eft->secf/dot_general | solution.py:77
  210.5 0.0 copy-done.1
  210.5 0.1 copy-done.4
  210.6 3.0 fusion.6
  213.6 0.0 copy-start.2
  213.6 0.0 copy-start.5
  213.6 0.0 all-gather.2.cloned.1.call-update
  213.7 63.9 %all-gather.2.cloned.1.call-done = bf16[32,1,32,2048]{3,2,0,1:T(8,128)(2,1)} async-done(((bf16[32,1,32,128]{3,2,0,1:T(8,128)(2,1)}), bf16[32,1,32,2048]{3,2,0,1:T(8,128)(2,1)}) %all-gather.2.cloned.1.call-update) | async-done | bytes 4194320 | tf_op jit(solution)/shard_map/all_gather | solution.py:82
  277.5 0.0 copy-done
  277.5 3.4 fusion.2
  281.0 4.2 %all_to_all.38 = bf16[16,2,32,256]{3,2,0,1:T(8,128)(2,1)S(1)} all-to-all(bf16[16,2,32,256]{3,2,0,1:T(8,128)(2,1)S(1)} %copy.45), channel_id=1, replica_groups=mesh['ep'=16,'tp_0'=16,'tp_1'=2] {'tp_1'}, dimensions={1} | all-to-all | bytes 1048576 | tf_op jit(solution)/shard_map/all_to_all | solution.py:36
  285.2 0.8 copy.46
  286.0 12.7 %all-to-all-start.4 = ((bf16[16,2,32,256]{3,2,1,0:T(8,128)(2,1)}), bf16[16,2,32,256]{3,2,1,0:T(8,128)(2,1)S(1)}, u32[]{:S(2)}, u32[]{:S(2)}) async-start(bf16[16,2,32,256]{3,2,1,0:T(8,128)(2,1)} %copy.46), calls=%async_computation.4 | async-start | bytes 1048576 | tf_op jit(solution)/shard_map/all_to_all | solution.py:36
  298.7 0.0 copy-done.2
  298.7 0.1 copy.47
  298.8 29.2 %all-to-all-done.4 = bf16[16,2,32,256]{3,2,1,0:T(8,128)(2,1)S(1)} async-done(((bf16[16,2,32,256]{3,2,1,0:T(8,128)(2,1)}), bf16[16,2,32,256]{3,2,1,0:T(8,128)(2,1)S(1)}, u32[]{:S(2)}, u32[]{:S(2)}) %all-to-all-start.4) | async-done | bytes 524320 | tf_op jit(solution)/shard_map/all_to_all | solution.py:36
  328.1 1.9 gather_fusion
  330.0 0.3 reshape.154
  330.3 0.7 multiply_reduce_fusion
  331.0 0.1 multiply_reduce_fusion.1
  331.1 0.6 broadcast_in_dim.8
  331.7 4.9 %all-to-all-start.5 = ((f32[16,1,256]{2,1,0:T(1,128)}), f32[16,1,256]{2,1,0:T(1,128)S(1)}, u32[]{:S(2)}, u32[]{:S(2)}) async-start(f32[16,1,256]{2,1,0:T(1,128)} %broadcast_in_dim.8), calls=%async_computation.5 | async-start | bytes 32768 | tf_op jit(solution)/shard_map/all_to_all | solution.py:13
  336.7 0.0 copy-done.5
  336.7 7.6 %all-to-all-done.5 = f32[16,1,256]{2,1,0:T(1,128)S(1)} async-done(((f32[16,1,256]{2,1,0:T(1,128)}), f32[16,1,256]{2,1,0:T(1,128)S(1)}, u32[]{:S(2)}, u32[]{:S(2)}) %all-to-all-start.5) | async-done | bytes 16416 | tf_op jit(solution)/shard_map/all_to_all | solution.py:13
  344.3 0.8 multiply_convert_fusion
  (13 shorter events, 0.2 us)
Async XLA Ops:
  6.5 271.0 %copy-start = (bf16[1,2048,256]{2,1,0:T(8,128)(2,1)S(1)}, bf16[1,2048,256]{2,1,0:T(8,128)(2,1)}, u32[]{:S(2)}) copy-start(bf16[1,2048,256]{2,1,0:T(8,128)(2,1)} %param.14) | copy-start | bytes 3145732
  8.3 14.6 %all-to-all-start = ((f32[16,1,256]{2,1,0:T(1,128)}), f32[16,1,256]{2,1,0:T(1,128)S(1)}, u32[]{:S(2)}, u32[]{:S(2)}) async-start(f32[16,1,256]{2,1,0:T(1,128)} %broadcast_in_dim.7), calls=%async_computation | async-start | bytes 32768 | tf_op jit(solution)/shard_map/all_to_all | solution.py:13
  15.3 262.2 %all-gather.2.cloned.1.call-start = ((), (), s32[]{:S(2)}) async-start(), calls=%async_computation.6 | async-start | bytes 4456448 | tf_op jit(solution)/shard_map/all_gather | solution.py:82
  191.0 13.6 %copy-start.3 = (bf16[1,128,4096]{2,1,0:T(8,128)(2,1)S(1)}, bf16[1,128,4096]{2,1,0:T(8,128)(2,1)}, u32[]{:S(2)}) copy-start(bf16[1,128,4096]{2,1,0:T(8,128)(2,1)} %param.12) | copy-start | bytes 3145732
  204.6 5.9 %copy-start.1 = (bf16[32,32,4096]{2,1,0:T(8,128)(2,1)S(1)}, bf16[32,32,4096]{2,1,0:T(8,128)(2,1)}, u32[]{:S(2)}) copy-start(bf16[32,32,4096]{2,1,0:T(8,128)(2,1)} %reshape.149) | copy-start | bytes 25165828
  204.6 6.0 %copy-start.4 = (bf16[1,128,4096]{2,1,0:T(8,128)(2,1)S(1)}, bf16[1,128,4096]{2,1,0:T(8,128)(2,1)}, u32[]{:S(2)}) copy-start(bf16[1,128,4096]{2,1,0:T(8,128)(2,1)} %param.13) | copy-start | bytes 3145732
  213.6 85.0 %copy-start.2 = (f32[256,2]{0,1:T(2,128)S(1)}, f32[256,2]{0,1:T(2,128)}, u32[]{:S(2)}) copy-start(f32[256,2]{0,1:T(2,128)} %param.11) | copy-start | bytes 6148
  213.6 123.0 %copy-start.5 = (bf16[256]{0:T(256)(128)(2,1)S(1)}, bf16[256]{0:T(256)(128)(2,1)}, u32[]{:S(2)}) copy-start(bf16[256]{0:T(256)(128)(2,1)} %param.15) | copy-start | bytes 1540
  286.0 42.1 %all-to-all-start.4 = ((bf16[16,2,32,256]{3,2,1,0:T(8,128)(2,1)}), bf16[16,2,32,256]{3,2,1,0:T(8,128)(2,1)S(1)}, u32[]{:S(2)}, u32[]{:S(2)}) async-start(bf16[16,2,32,256]{3,2,1,0:T(8,128)(2,1)} %copy.46), calls=%async_computation.4 | async-start | bytes 1048576 | tf_op jit(solution)/shard_map/all_to_all | solution.py:36
  331.7 12.5 %all-to-all-start.5 = ((f32[16,1,256]{2,1,0:T(1,128)}), f32[16,1,256]{2,1,0:T(1,128)S(1)}, u32[]{:S(2)}, u32[]{:S(2)}) async-start(f32[16,1,256]{2,1,0:T(1,128)} %broadcast_in_dim.8), calls=%async_computation.5 | async-start | bytes 32768 | tf_op jit(solution)/shard_map/all_to_all | solution.py:13
Sparse Core Ops, SparseCore 0:
  213.8 63.7 all-gather.1
